TPU v7x, 32 devices: a whole 2x2x4 slice. The times are simulated.
32 devices in a mesh: rep: 2 (over x), fs: 8 (over z, y), tp: 2 (over core).
Axes of the slice: x: 2, y: 2, z: 4, core: 2. Of those that a mesh axis runs over, the one named last changes fastest.
Arguments:
- tokens: bfloat16 [256, 16, 2048], P('tp', ('rep', 'fs')), may hold values from -6 to 6
- mix_gain: float32 [2048], replicated, may hold values from 0.1 to 1.9
- value_weight: bfloat16 [2048, 1024], P('fs', 'tp'), may hold values from -0.125 to 0.125
- gate_weight: bfloat16 [2048, 1024], P('fs', 'tp'), may hold values from -0.125 to 0.125
- conv_taps: float32 [31, 1024], P(None, 'tp'), may hold values from -1 to 1
- head_gain: float32 [1024], P('tp'), may hold values from 0.1 to 1.9
- out_weight: bfloat16 [1024, 2048], P('tp', 'fs'), may hold values from -0.1875 to 0.1875
- ffn_gain: float32 [2048], replicated, may hold values from 0.1 to 1.9
- ffn_gate_weight: bfloat16 [2048, 3072], P('fs', 'tp'), may hold values from -0.125 to 0.125
- ffn_up_weight: bfloat16 [2048, 3072], P('fs', 'tp'), may hold values from -0.125 to 0.125
- down_weight: bfloat16 [3072, 2048], P('tp', 'fs'), may hold values from -0.109375 to 0.109375
Outputs:
- layer_out: bfloat16 [256, 16, 2048], P('tp', ('rep', 'fs'))
All inputs are finite; a program needn't handle non-finite values.
Results may differ from a plain program's by a relative error of at most 0.012.
Values may be sent and summed in bfloat16 or wider, within the bound.
A program may use at most 128 MiB of HBM per device.

v0:
```python
import jax
import jax.numpy as jnp
from jax import lax
from jax.sharding import PartitionSpec as P

HEAD_DIM = 128
norm_eps = 1e-06
group_eps = 1e-05


def rms_scale(matrix, scales):
    return matrix * lax.rsqrt(jnp.mean(matrix * matrix, axis=-1, keepdims=True) + norm_eps) * scales


def body(
    tokens,
    mix_gain,
    value_weight,
    gate_weight,
    conv_taps,
    head_gain,
    out_weight,
    ffn_gain,
    ffn_gate_weight,
    ffn_up_weight,
    down_weight,
):
    local_len, seq_count, model_width = tokens.shape
    own_rows = local_len * seq_count
    whole_rows = lax.all_gather(tokens, "tp", axis=0, tiled=True)
    full_len = whole_rows.shape[0]
    normed = rms_scale(whole_rows.reshape(-1, model_width).astype(jnp.float32), mix_gain).astype(
        jnp.bfloat16
    )
    channels = value_weight.shape[1]
    pieces = (
        lax.all_gather(value_weight, "fs", axis=0, tiled=True),
        lax.all_gather(gate_weight, "fs", axis=0, tiled=True),
    )
    sliced = normed
    value_rows = jnp.dot(sliced, pieces[0], preferred_element_type=jnp.float32)
    gate_rows = jnp.dot(sliced, pieces[1], preferred_element_type=jnp.float32)
    glu_rows = (
        (value_rows * jax.nn.sigmoid(gate_rows))
        .astype(jnp.bfloat16)
        .reshape(full_len, seq_count, channels)
    )
    kernel = conv_taps.shape[0]
    conved = lax.conv_general_dilated(
        glu_rows.astype(jnp.float32),
        conv_taps[:, None, :],
        (1,),
        [(kernel // 2, kernel // 2)],
        dimension_numbers=("WNC", "WIO", "WNC"),
        feature_group_count=channels,
        precision=lax.Precision.HIGHEST,
    )
    grouped = conved.reshape(full_len, seq_count, channels // HEAD_DIM, HEAD_DIM)
    head_mean = jnp.mean(grouped, axis=-1, keepdims=True)
    head_var = jnp.mean(jnp.square(grouped - head_mean), axis=-1, keepdims=True)
    scaled = (
        (grouped - head_mean) * lax.rsqrt(head_var + group_eps) * head_gain.reshape(-1, HEAD_DIM)
    )
    activated = jax.nn.silu(scaled).astype(jnp.bfloat16).reshape(-1, channels)
    out_columns = lax.all_gather(out_weight, "fs", axis=1, tiled=True)
    sliced = lax.slice_in_dim(activated, 0, own_rows * lax.axis_size("tp"), axis=0)
    mixed_rows = lax.psum_scatter(
        jnp.dot(sliced, out_columns, preferred_element_type=jnp.float32).astype(jnp.bfloat16),
        "tp",
        scatter_dimension=0,
        tiled=True,
    ).astype(jnp.float32)
    residual = tokens.reshape(own_rows, model_width).astype(jnp.float32)
    middle = (residual + mixed_rows).astype(jnp.bfloat16)
    middle_whole = lax.all_gather(
        middle.reshape(local_len, seq_count, model_width), "tp", axis=0, tiled=True
    )
    normed_ffn = rms_scale(
        middle_whole.reshape(-1, model_width).astype(jnp.float32), ffn_gain
    ).astype(jnp.bfloat16)
    pieces = (
        lax.all_gather(ffn_gate_weight, "fs", axis=0, tiled=True),
        lax.all_gather(ffn_up_weight, "fs", axis=0, tiled=True),
    )
    sliced = normed_ffn
    gate_part = jnp.dot(sliced, pieces[0], preferred_element_type=jnp.float32)
    up_part = jnp.dot(sliced, pieces[1], preferred_element_type=jnp.float32)
    hidden = (jax.nn.silu(gate_part) * up_part).astype(jnp.bfloat16)
    down_columns = lax.all_gather(down_weight, "fs", axis=1, tiled=True)
    sliced = hidden
    fed_rows = lax.psum_scatter(
        jnp.dot(sliced, down_columns, preferred_element_type=jnp.float32).astype(jnp.bfloat16),
        "tp",
        scatter_dimension=0,
        tiled=True,
    ).astype(jnp.float32)
    layer_rows = (middle.astype(jnp.float32) + fed_rows).astype(jnp.bfloat16)
    return layer_rows.reshape(local_len, seq_count, model_width)


def solution(mesh):
    placed = (
        P("tp", ("rep", "fs"), None),
        P(),
        P("fs", "tp"),
        P("fs", "tp"),
        P(None, "tp"),
        P("tp"),
        P("tp", "fs"),
        P(),
        P("fs", "tp"),
        P("fs", "tp"),
        P("tp", "fs"),
    )
    return jax.shard_map(
        body, mesh=mesh, in_specs=placed, out_specs=P("tp", ("rep", "fs"), None), check_vma=False
    )
```

profile of v0, /device:TPU:0, one launch (start us, length us, event | category | flops | bytes accessed | tf_op | source)
XLA Modules:
  0.0 522.6 jit_solution(14361909878251636009)
XLA Ops:
  6.5 0.7 all-gather.10.cloned.1.call-update
  7.3 0.0 all-gather.14.cloned.1.call-start
  7.3 0.7 all-gather.14.cloned.1.call-update
  8.0 0.0 all-gather.12.cloned.1.call-start
  8.1 0.7 all-gather.12.cloned.1.call-update
  8.7 0.0 all-gather.16.cloned.1.call-start
  8.8 0.5 all-gather.16.cloned.1.call-update
  9.3 0.0 reduce-scatter.3.cloned.1.call-start
  9.4 11.3 %all-gather.10.cloned.1.call-done = bf16[256,1,2048]{2,0,1:T(8,128)(2,1)} async-done(((bf16[128,1,2048]{2,0,1:T(8,128)(2,1)}), bf16[256,1,2048]{2,0,1:T(8,128)(2,1)}) %all-gather.10.cloned.1.call-update) | async-done | bytes 1048592 | tf_op jit(solution)/shard_map/all_gather | solution.py:30
  20.7 1.5 fusion.4
  22.2 50.9 %all-gather.14.cloned.1.call-done = bf16[2048,512]{1,0:T(8,128)(2,1)} async-done(((bf16[256,512]{1,0:T(8,128)(2,1)}), bf16[2048,512]{1,0:T(8,128)(2,1)}) %all-gather.14.cloned.1.call-update) | async-done | bytes 2097168 | tf_op jit(solution)/shard_map/all_gather | solution.py:38
  73.1 2.8 fusion.9
  75.8 47.0 %all-gather.12.cloned.1.call-done = bf16[2048,512]{1,0:T(8,128)(2,1)} async-done(((bf16[256,512]{1,0:T(8,128)(2,1)}), bf16[2048,512]{1,0:T(8,128)(2,1)}) %all-gather.12.cloned.1.call-update) | async-done | bytes 2097168 | tf_op jit(solution)/shard_map/all_gather | solution.py:37
  122.9 2.3 fusion.11
  125.2 0.1 pad
  125.3 0.1 reshape.110
  125.4 0.1 copy.17
  125.5 0.1 slice.2
  125.5 0.4 copy-done.8
  125.9 1.3 convolution_select_fusion
  127.2 0.3 copy.19
  127.5 0.1 reshape.114
  127.7 0.2 reshape.104
  127.9 0.2 reshape.105
  128.1 0.3 reduce_sum.37
  128.4 0.6 multiply_reduce_fusion
  129.1 44.6 %all-gather.16.cloned.1.call-done = bf16[512,2048]{1,0:T(8,128)(2,1)} async-done(((bf16[512,256]{1,0:T(8,128)(2,1)}), bf16[512,2048]{1,0:T(8,128)(2,1)}) %all-gather.16.cloned.1.call-update) | async-done | bytes 2097168 | tf_op jit(solution)/shard_map/all_gather | solution.py:65
  173.7 0.3 mul.85
  174.0 0.3 sub.31
  174.4 3.4 convolution_convert_fusion
  177.8 0.0 all-gather.24.cloned.1.call-start
  177.8 6.7 %reduce-scatter.3.cloned.1.call-done = bf16[128,2048]{1,0:T(8,128)(2,1)} async-done(((bf16[256,2048]{1,0:T(8,128)(2,1)}), bf16[128,2048]{1,0:T(8,128)(2,1)}) %reduce-scatter.3.cloned.1.call-update) | async-done | bytes 524304 | tf_op jit(solution)/shard_map/reduce_scatter | solution.py:67
  184.5 2.0 fusion.13
  186.5 0.0 all-gather.18.cloned.1.call-start
  186.5 0.7 all-gather.18.cloned.1.call-update
  187.2 0.0 all-gather.20.cloned.1.call-start
  187.3 0.7 all-gather.20.cloned.1.call-update
  188.0 0.7 all-gather.22.cloned.1.call-update
  188.7 0.0 reduce-scatter.5.cloned.1.call-start
  188.8 8.1 %all-gather.24.cloned.1.call-done = bf16[256,2048]{1,0:T(8,128)(2,1)} async-done(((bf16[128,2048]{1,0:T(8,128)(2,1)}), bf16[256,2048]{1,0:T(8,128)(2,1)}) %all-gather.24.cloned.1.call-update) | async-done | bytes 1048592 | tf_op jit(solution)/shard_map/all_gather | solution.py:75
  196.9 1.5 fusion.3
  198.4 100.6 %all-gather.18.cloned.1.call-done = bf16[2048,1536]{1,0:T(8,128)(2,1)} async-done(((bf16[256,1536]{1,0:T(8,128)(2,1)}), bf16[2048,1536]{1,0:T(8,128)(2,1)}) %all-gather.18.cloned.1.call-update) | async-done | bytes 6291472 | tf_op jit(solution)/shard_map/all_gather | solution.py:82
  299.0 5.0 fusion.26
  303.9 94.1 %all-gather.20.cloned.1.call-done = bf16[2048,1536]{1,0:T(8,128)(2,1)} async-done(((bf16[256,1536]{1,0:T(8,128)(2,1)}), bf16[2048,1536]{1,0:T(8,128)(2,1)}) %all-gather.20.cloned.1.call-update) | async-done | bytes 6291472 | tf_op jit(solution)/shard_map/all_gather | solution.py:83
  398.1 99.7 %all-gather.22.cloned.1.call-done = bf16[1536,2048]{1,0:T(8,128)(2,1)} async-done(((bf16[1536,256]{1,0:T(8,128)(2,1)}), bf16[1536,2048]{1,0:T(8,128)(2,1)}) %all-gather.22.cloned.1.call-update) | async-done | bytes 6291472 | tf_op jit(solution)/shard_map/all_gather | solution.py:89
  497.8 9.3 %convolution_convert_fusion.1 = bf16[256,2048]{1,0:T(8,128)(2,1)} fusion(bf16[1536,2048]{1,0:T(8,128)(2,1)} %all-gather.22.cloned.1.call-done, bf16[2048,1536]{1,0:T(8,128)(2,1)} %all-gather.20.cloned.1.call-done, f32[256,1536]{1,0:T(8,128)S(1)} %fusion.26, bf16[256,2048]{1,0:T(8,128)(2,1)S(1)} %copy-done.3, f32[2048]{0:T(1024)S(1)} %copy-done.6, ...), kind=kOutput, calls=%fused_computation.7 | convolution fusion | flops 3226206208 | bytes 16262144 | tf_op jit(solution)/shard_map/dot_general | solution.py:92
  507.1 6.7 %reduce-scatter.5.cloned.1.call-done = bf16[128,2048]{1,0:T(8,128)(2,1)} async-done(((bf16[256,2048]{1,0:T(8,128)(2,1)}), bf16[128,2048]{1,0:T(8,128)(2,1)}) %reduce-scatter.5.cloned.1.call-update) | async-done | bytes 524304 | tf_op jit(solution)/shard_map/reduce_scatter | solution.py:91
  513.8 2.0 fusion.20
  (27 shorter events, 0.2 us)
Async XLA Ops:
  6.5 119.0 %copy-start = (f32[31,512]{1,0:T(8,128)S(1)}, f32[31,512]{1,0:T(8,128)}, u32[]{:S(2)}) copy-start(f32[31,512]{1,0:T(8,128)} %param.15) | copy-start | bytes 190468
  6.5 66.5 %copy-start.5 = (f32[2048]{0:T(1024)S(1)}, f32[2048]{0:T(1024)}, u32[]{:S(2)}) copy-start(f32[2048]{0:T(1024)} %param.12) | copy-start | bytes 24580
  6.5 14.1 %all-gather.10.cloned.1.call-start = ((), (), s32[]{:S(2)}) async-start(), calls=%async_computation.2 | async-start | bytes 1572864 | tf_op jit(solution)/shard_map/all_gather | solution.py:30
  7.3 65.8 %all-gather.14.cloned.1.call-start = ((), (), s32[]{:S(2)}) async-start(), calls=%async_computation.4 | async-start | bytes 2359296 | tf_op jit(solution)/shard_map/all_gather | solution.py:38
  8.0 114.9 %all-gather.12.cloned.1.call-start = ((), (), s32[]{:S(2)}) async-start(), calls=%async_computation.3 | async-start | bytes 2359296 | tf_op jit(solution)/shard_map/all_gather | solution.py:37
  8.7 164.9 %all-gather.16.cloned.1.call-start = ((), (), s32[]{:S(2)}) async-start(), calls=%async_computation.5 | async-start | bytes 2359296 | tf_op jit(solution)/shard_map/all_gather | solution.py:65
  9.3 175.2 %reduce-scatter.3.cloned.1.call-start = ((), (), s32[]{:S(2)}) async-start(), calls=%async_computation.6 | async-start | bytes 1572864 | tf_op jit(solution)/shard_map/reduce_scatter | solution.py:67
  22.2 100.7 %copy-start.4 = (bf16[256,1,2048]{2,0,1:T(8,128)(2,1)S(1)}, bf16[256,1,2048]{2,0,1:T(8,128)(2,1)}, u32[]{:S(2)}) copy-start(bf16[256,1,2048]{2,0,1:T(8,128)(2,1)} %all-gather.10.cloned.1.call-done) | copy-start | bytes 3145732
  125.2 0.7 copy-start.8
  127.8 46.5 %copy-start.7 = (f32[512]{0:T(512)S(1)}, f32[512]{0:T(512)}, u32[]{:S(2)}) copy-start(f32[512]{0:T(512)} %param.16) | copy-start | bytes 6148
  174.3 10.2 %copy-start.2 = (bf16[128,1,2048]{2,0,1:T(8,128)(2,1)S(1)}, bf16[128,1,2048]{2,0,1:T(8,128)(2,1)}, u32[]{:S(2)}) copy-start(bf16[128,1,2048]{2,0,1:T(8,128)(2,1)} %param.11) | copy-start | bytes 1572868
  177.8 19.1 %all-gather.24.cloned.1.call-start = ((), (), s32[]{:S(2)}) async-start(), calls=%async_computation.11 | async-start | bytes 1572864 | tf_op jit(solution)/shard_map/all_gather | solution.py:75
  186.5 112.5 %copy-start.6 = (f32[2048]{0:T(1024)S(1)}, f32[2048]{0:T(1024)}, u32[]{:S(2)}) copy-start(f32[2048]{0:T(1024)} %param.18) | copy-start | bytes 24580
  186.5 112.5 %all-gather.18.cloned.1.call-start = ((), (), s32[]{:S(2)}) async-start(), calls=%async_computation.7 | async-start | bytes 7077888 | tf_op jit(solution)/shard_map/all_gather | solution.py:82
  187.2 210.8 %all-gather.20.cloned.1.call-start = ((), (), s32[]{:S(2)}) async-start(), calls=%async_computation.8 | async-start | bytes 7077888 | tf_op jit(solution)/shard_map/all_gather | solution.py:83
  188.0 309.8 %all-gather.22.cloned.1.call-start = ((), (), s32[]{:S(2)}) async-start(), calls=%async_computation.9 | async-start | bytes 7077888 | tf_op jit(solution)/shard_map/all_gather | solution.py:89
  188.7 325.1 %reduce-scatter.5.cloned.1.call-start = ((), (), s32[]{:S(2)}) async-start(), calls=%async_computation.10 | async-start | bytes 1572864 | tf_op jit(solution)/shard_map/reduce_scatter | solution.py:91
  198.4 299.4 %copy-start.3 = (bf16[256,2048]{1,0:T(8,128)(2,1)S(1)}, bf16[256,2048]{1,0:T(8,128)(2,1)}, u32[]{:S(2)}) copy-start(bf16[256,2048]{1,0:T(8,128)(2,1)} %all-gather.24.cloned.1.call-done) | copy-start | bytes 3145732
  303.9 209.9 %copy-start.1 = (bf16[128,2048]{1,0:T(8,128)(2,1)S(1)}, bf16[128,2048]{1,0:T(8,128)(2,1)}, u32[]{:S(2)}) copy-start(bf16[128,2048]{1,0:T(8,128)(2,1)} %fusion.13) | copy-start | bytes 1572868
Sparse Core Ops, SparseCore 0:
  8.9 11.7 all-gather.9
  22.8 50.2 all-gather.13
  75.2 47.6 all-gather.11
  124.8 48.8 all-gather.15
  177.9 6.5 reduce-scatter.2
  186.6 10.2 all-gather.23
  199.1 99.8 all-gather.17
  301.1 96.8 all-gather.19
  400.1 97.6 all-gather.21
  507.2 6.5 reduce-scatter.4
where the time goes:
time: 523 us
  waiting for transfers between devices  474 us (91%)
  matrix products  24 us (5%)
  between operations  13.7 us (3%)
  other arithmetic  7.98 us (2%)
    all_gather x1, waiting for transfers between devices, body(): lax.all_gather(ffn_gate_weight, 'fs', axis=0, tiled=True)  101 us
    all_gather x1, waiting for transfers between devices, body(): down_columns = lax.all_gather(down_weight, 'fs', axis=1, tiled=True)  99.7 us
    all_gather x1, waiting for transfers between devices, body(): lax.all_gather(ffn_up_weight, 'fs', axis=0, tiled=True)  94.1 us
    all_gather x1, waiting for transfers between devices, body(): lax.all_gather(gate_weight, 'fs', axis=0, tiled=True)  50.9 us
    all_gather x1, waiting for transfers between devices, body(): lax.all_gather(value_weight, 'fs', axis=0, tiled=True)  47 us
    all_gather x1, waiting for transfers between devices, body(): out_columns = lax.all_gather(out_weight, 'fs', axis=1, tiled=True)  44.6 us
    all_gather x1, waiting for transfers between devices, body(): whole_rows = lax.all_gather(tokens, 'tp', axis=0, tiled=True)  11.3 us
  transfers between devices with their start and end apart: 10, of which 10 were waited for; matrix products, arithmetic and copies ran while one was open for 3% of the time, Pallas kernels for 0%

commit v1 on v0

--- a/solution.py
+++ b/solution.py
@@ -62,7 +62,12 @@
         (grouped - head_mean) * lax.rsqrt(head_var + group_eps) * head_gain.reshape(-1, HEAD_DIM)
     )
     activated = jax.nn.silu(scaled).astype(jnp.bfloat16).reshape(-1, channels)
-    out_columns = lax.all_gather(out_weight, "fs", axis=1, tiled=True)
+    ring = [out_weight]
+    for hop in range(7):
+        ring.append(lax.ppermute(ring[-1], "fs", [(dev, (dev + 1) % 8) for dev in range(8)]))
+    out_columns = jnp.roll(
+        jnp.concatenate(ring[::-1], axis=1), (lax.axis_index("fs") + 1) * ring[0].shape[1], axis=1
+    )
     sliced = lax.slice_in_dim(activated, 0, own_rows * lax.axis_size("tp"), axis=0)
     mixed_rows = lax.psum_scatter(
         jnp.dot(sliced, out_columns, preferred_element_type=jnp.float32).astype(jnp.bfloat16),

time: 523 us -> 493 us (0.943)
  waiting for transfers between devices: 474 us -> 430 us
  local copies, waits for them, and re-layouts: 2.15 us -> 13.8 us
    ppermute x0 -> x7, waiting for transfers between devices: none -> 83.6 us  [body(): lax.ppermute(ring[-1], 'fs', [(dev, (dev + 1) % 8) for dev in range(8)])]
    all_gather x1, waiting for transfers between devices: 50.9 us -> 0.01 us  [body(): lax.all_gather(gate_weight, 'fs', axis=0, tiled=True)]
    all_gather x1 -> x0, waiting for transfers between devices: 44.6 us -> none  [body(): out_columns = lax.all_gather(out_weight, 'fs', axis=1, tiled=True)]
    all_gather x1, waiting for transfers between devices: 47 us -> 26.6 us  [body(): lax.all_gather(value_weight, 'fs', axis=0, tiled=True)]
    all_gather x1, waiting for transfers between devices: 11.3 us -> 0.01 us  [body(): whole_rows = lax.all_gather(tokens, 'tp', axis=0, tiled=True)]
    unnamed x18 -> x35, local copies, waits for them, and re-layouts: 0.41 us -> 11.3 us
  transfers between devices with their start and end apart: 10 -> 16, of which waited for: 10 -> 14; matrix products, arithmetic and copies ran while one was open for 3% -> 5% of each run, Pallas kernels for 0% -> 0%
where the time goes in v1:
time: 493 us; the launch traced here: 492 us
  waiting for transfers between devices  430 us (87%)
  matrix products  23.7 us (5%)
  local copies, waits for them, and re-layouts  13.8 us (3%)
  between operations  13.4 us (3%)
  other arithmetic  7.97 us (2%)
    all_gather x1, waiting for transfers between devices, body(): lax.all_gather(ffn_gate_weight, 'fs', axis=0, tiled=True)  100 us
    all_gather x1, waiting for transfers between devices, body(): down_columns = lax.all_gather(down_weight, 'fs', axis=1, tiled=True)  99.7 us
    all_gather x1, waiting for transfers between devices, body(): lax.all_gather(ffn_up_weight, 'fs', axis=0, tiled=True)  94.1 us
    ppermute x7, waiting for transfers between devices, body(): lax.ppermute(ring[-1], 'fs', [(dev, (dev + 1) % 8) for dev in range(8)])  83.6 us
    all_gather x1, waiting for transfers between devices, body(): lax.all_gather(value_weight, 'fs', axis=0, tiled=True)  26.6 us
    unnamed x35, local copies, waits for them, and re-layouts  11.3 us
  transfers between devices with their start and end apart: 16, of which 14 were waited for; matrix products, arithmetic and copies ran while one was open for 5% of the time, Pallas kernels for 0%

profile of v1, /device:TPU:0, one launch (start us, length us, event | category | flops | bytes accessed | tf_op | source)
XLA Modules:
  0.0 492.1 jit_solution(1834050734006623645)
XLA Ops:
  6.5 0.7 all-gather.9.cloned.1.call-update
  7.3 0.7 all-gather.13.cloned.1.call-update
  8.1 3.0 collective-permute-start
  11.1 9.6 %collective-permute-done = bf16[512,256]{1,0:T(8,128)(2,1)S(1)} collective-permute-done((bf16[512,256]{1,0:T(8,128)(2,1)}, bf16[512,256]{1,0:T(8,128)(2,1)S(1)}, u32[]{:S(2)}, u32[]{:S(2)}) %collective-permute-start) | collective-permute-done | bytes 262176 | tf_op jit(solution)/shard_map/ppermute | solution.py:67
  20.7 10.2 %collective-permute-done.1 = bf16[512,256]{1,0:T(8,128)(2,1)S(1)} collective-permute-done((bf16[512,256]{1,0:T(8,128)(2,1)S(1)}, bf16[512,256]{1,0:T(8,128)(2,1)S(1)}, u32[]{:S(2)}, u32[]{:S(2)}) %collective-permute-start.1) | collective-permute-done | bytes 262176 | tf_op jit(solution)/shard_map/ppermute | solution.py:67
  30.9 15.0 %collective-permute-done.2 = bf16[512,256]{1,0:T(8,128)(2,1)S(1)} collective-permute-done((bf16[512,256]{1,0:T(8,128)(2,1)S(1)}, bf16[512,256]{1,0:T(8,128)(2,1)S(1)}, u32[]{:S(2)}, u32[]{:S(2)}) %collective-permute-start.2) | collective-permute-done | bytes 262176 | tf_op jit(solution)/shard_map/ppermute | solution.py:67
  45.9 9.1 %collective-permute-done.3 = bf16[512,256]{1,0:T(8,128)(2,1)S(1)} collective-permute-done((bf16[512,256]{1,0:T(8,128)(2,1)S(1)}, bf16[512,256]{1,0:T(8,128)(2,1)S(1)}, u32[]{:S(2)}, u32[]{:S(2)}) %collective-permute-start.3) | collective-permute-done | bytes 262176 | tf_op jit(solution)/shard_map/ppermute | solution.py:67
  55.0 16.4 %collective-permute-done.4 = bf16[512,256]{1,0:T(8,128)(2,1)S(1)} collective-permute-done((bf16[512,256]{1,0:T(8,128)(2,1)S(1)}, bf16[512,256]{1,0:T(8,128)(2,1)S(1)}, u32[]{:S(2)}, u32[]{:S(2)}) %collective-permute-start.4) | collective-permute-done | bytes 262176 | tf_op jit(solution)/shard_map/ppermute | solution.py:67
  71.3 15.9 %collective-permute-done.5 = bf16[512,256]{1,0:T(8,128)(2,1)S(1)} collective-permute-done((bf16[512,256]{1,0:T(8,128)(2,1)S(1)}, bf16[512,256]{1,0:T(8,128)(2,1)S(1)}, u32[]{:S(2)}, u32[]{:S(2)}) %collective-permute-start.5) | collective-permute-done | bytes 262176 | tf_op jit(solution)/shard_map/ppermute | solution.py:67
  87.3 1.5 fusion.4
  88.8 7.5 %collective-permute-done.6 = bf16[512,256]{1,0:T(8,128)(2,1)S(1)} collective-permute-done((bf16[512,256]{1,0:T(8,128)(2,1)S(1)}, bf16[512,256]{1,0:T(8,128)(2,1)S(1)}, u32[]{:S(2)}, u32[]{:S(2)}) %collective-permute-start.6) | collective-permute-done | bytes 262176 | tf_op jit(solution)/shard_map/ppermute | solution.py:67
  96.3 0.7 constant_dynamic-update-slice_fusion.15
  97.1 0.8 constant_dynamic-update-slice_fusion.14
  97.8 0.8 constant_dynamic-update-slice_fusion.13
  98.6 0.7 constant_dynamic-update-slice_fusion.12
  99.3 0.8 constant_dynamic-update-slice_fusion.11
  100.1 0.7 constant_dynamic-update-slice_fusion.10
  100.8 0.7 constant_dynamic-update-slice_fusion.9
  101.6 0.8 constant_dynamic-update-slice_fusion.8
  102.3 0.7 constant_dynamic-update-slice_fusion.7
  103.1 0.8 constant_dynamic-update-slice_fusion.6
  103.9 0.8 constant_dynamic-update-slice_fusion.5
  104.6 0.8 constant_dynamic-update-slice_fusion.4
  105.4 0.8 constant_dynamic-update-slice_fusion.3
  106.2 0.7 constant_dynamic-update-slice_fusion.2
  106.9 0.7 constant_dynamic-update-slice_fusion.1
  107.6 0.7 constant_dynamic-update-slice_fusion
  108.4 2.4 fusion.10
  110.8 26.6 %all-gather.11.cloned.1.call-done = bf16[2048,512]{1,0:T(8,128)(2,1)} async-done(((bf16[256,512]{1,0:T(8,128)(2,1)}), bf16[2048,512]{1,0:T(8,128)(2,1)}) %all-gather.11.cloned.1.call-update) | async-done | bytes 2097168 | tf_op jit(solution)/shard_map/all_gather | solution.py:37
  137.4 2.3 fusion.12
  140.1 1.3 convolution_select_fusion
  141.4 0.3 copy.19
  142.6 0.6 multiply_reduce_fusion
  143.9 3.4 convolution_convert_fusion
  147.4 7.0 %reduce-scatter.3.cloned.1.call-done = bf16[128,2048]{1,0:T(8,128)(2,1)} async-done(((bf16[256,2048]{1,0:T(8,128)(2,1)}), bf16[128,2048]{1,0:T(8,128)(2,1)}) %reduce-scatter.3.cloned.1.call-update) | async-done | bytes 524304 | tf_op jit(solution)/shard_map/reduce_scatter | solution.py:72
  154.4 2.0 fusion.14
  156.4 0.5 all-gather.15.cloned.1.call-update
  157.0 0.7 all-gather.17.cloned.1.call-update
  157.8 0.7 all-gather.19.cloned.1.call-update
  158.7 8.1 %all-gather.21.cloned.1.call-done = bf16[256,2048]{1,0:T(8,128)(2,1)} async-done(((bf16[128,2048]{1,0:T(8,128)(2,1)}), bf16[256,2048]{1,0:T(8,128)(2,1)}) %all-gather.21.cloned.1.call-update) | async-done | bytes 1048592 | tf_op jit(solution)/shard_map/all_gather | solution.py:80
  166.8 1.5 fusion.3
  168.3 100.4 %all-gather.15.cloned.1.call-done = bf16[2048,1536]{1,0:T(8,128)(2,1)} async-done(((bf16[256,1536]{1,0:T(8,128)(2,1)}), bf16[2048,1536]{1,0:T(8,128)(2,1)}) %all-gather.15.cloned.1.call-update) | async-done | bytes 6291472 | tf_op jit(solution)/shard_map/all_gather | solution.py:87
  268.8 5.0 %fusion.27 = f32[256,1536]{1,0:T(8,128)S(1)} fusion(bf16[2048,1536]{1,0:T(8,128)(2,1)} %all-gather.15.cloned.1.call-done, bf16[256,2048]{1,0:T(8,128)(2,1)} %all-gather.21.cloned.1.call-done, f32[2048]{0:T(1024)S(1)} %copy-done.7, f32[256]{0:T(256)S(1)} %add_rsqrt_fusion.1), kind=kOutput, calls=%fused_computation.39 | convolution fusion | flops 1612709888 | bytes 8922112 | tf_op jit(solution)/shard_map/dot_general | solution.py:91
  273.7 94.1 %all-gather.17.cloned.1.call-done = bf16[2048,1536]{1,0:T(8,128)(2,1)} async-done(((bf16[256,1536]{1,0:T(8,128)(2,1)}), bf16[2048,1536]{1,0:T(8,128)(2,1)}) %all-gather.17.cloned.1.call-update) | async-done | bytes 6291472 | tf_op jit(solution)/shard_map/all_gather | solution.py:88
  367.8 99.7 %all-gather.19.cloned.1.call-done = bf16[1536,2048]{1,0:T(8,128)(2,1)} async-done(((bf16[1536,256]{1,0:T(8,128)(2,1)}), bf16[1536,2048]{1,0:T(8,128)(2,1)}) %all-gather.19.cloned.1.call-update) | async-done | bytes 6291472 | tf_op jit(solution)/shard_map/all_gather | solution.py:94
  467.6 9.3 %convolution_convert_fusion.1 = bf16[256,2048]{1,0:T(8,128)(2,1)} fusion(bf16[1536,2048]{1,0:T(8,128)(2,1)} %all-gather.19.cloned.1.call-done, bf16[2048,1536]{1,0:T(8,128)(2,1)} %all-gather.17.cloned.1.call-done, f32[256,1536]{1,0:T(8,128)S(1)} %fusion.27, bf16[256,2048]{1,0:T(8,128)(2,1)S(1)} %copy-done.4, f32[2048]{0:T(1024)S(1)} %copy-done.7, ...), kind=kOutput, calls=%fused_computation.7 | convolution fusion | flops 3226206208 | bytes 16262144 | tf_op jit(solution)/shard_map/dot_general | solution.py:97
  476.9 6.7 %reduce-scatter.5.cloned.1.call-done = bf16[128,2048]{1,0:T(8,128)(2,1)} async-done(((bf16[256,2048]{1,0:T(8,128)(2,1)}), bf16[128,2048]{1,0:T(8,128)(2,1)}) %reduce-scatter.5.cloned.1.call-update) | async-done | bytes 524304 | tf_op jit(solution)/shard_map/reduce_scatter | solution.py:96
  483.6 2.0 fusion.21
  (56 shorter events, 2.4 us)
Async XLA Ops:
  6.5 133.5 %copy-start = (f32[31,512]{1,0:T(8,128)S(1)}, f32[31,512]{1,0:T(8,128)}, u32[]{:S(2)}) copy-start(f32[31,512]{1,0:T(8,128)} %param.15) | copy-start | bytes 190468
  6.5 95.0 %copy-start.5 = (bf16[512,256]{1,0:T(8,128)(2,1)S(1)}, bf16[512,256]{1,0:T(8,128)(2,1)}, u32[]{:S(2)}) copy-start(bf16[512,256]{1,0:T(8,128)(2,1)} %param.17) | copy-start | bytes 786436
  6.5 80.7 %all-gather.9.cloned.1.call-start = ((), (), s32[]{:S(2)}) async-start(), calls=%async_computation.2 | async-start | bytes 1572864 | tf_op jit(solution)/shard_map/all_gather | solution.py:30
  7.3 101.1 %all-gather.13.cloned.1.call-start = ((), (), s32[]{:S(2)}) async-start(), calls=%async_computation.4 | async-start | bytes 2359296 | tf_op jit(solution)/shard_map/all_gather | solution.py:38
  8.0 129.4 %all-gather.11.cloned.1.call-start = ((), (), s32[]{:S(2)}) async-start(), calls=%async_computation.3 | async-start | bytes 2359296 | tf_op jit(solution)/shard_map/all_gather | solution.py:37
  8.1 12.6 %collective-permute-start = (bf16[512,256]{1,0:T(8,128)(2,1)}, bf16[512,256]{1,0:T(8,128)(2,1)S(1)}, u32[]{:S(2)}, u32[]{:S(2)}) collective-permute-start(bf16[512,256]{1,0:T(8,128)(2,1)} %param.17), channel_id=1, source_target_pairs={{0,2},{2,4},{4,6},{6,8},{8,10},{10,12},{12,14},{14,0},{1,3},{3,5},... | collective-permute-start | bytes 786440 | tf_op jit(solution)/shard_map/ppermute | solution.py:67
  20.7 10.2 %collective-permute-start.1 = (bf16[512,256]{1,0:T(8,128)(2,1)S(1)}, bf16[512,256]{1,0:T(8,128)(2,1)S(1)}, u32[]{:S(2)}, u32[]{:S(2)}) collective-permute-start(bf16[512,256]{1,0:T(8,128)(2,1)S(1)} %collective-permute-done), channel_id=1, source_target_pairs={{0,2},{2,4},{4,6},{6,8},{8,10},{10,12},{12,14},{14,0},{1,3},{3,5},... | collective-permute-start | bytes 786440 | tf_op jit(solution)/shard_map/ppermute | solution.py:67
  30.8 15.1 %collective-permute-start.2 = (bf16[512,256]{1,0:T(8,128)(2,1)S(1)}, bf16[512,256]{1,0:T(8,128)(2,1)S(1)}, u32[]{:S(2)}, u32[]{:S(2)}) collective-permute-start(bf16[512,256]{1,0:T(8,128)(2,1)S(1)} %collective-permute-done.1), channel_id=1, source_target_pairs={{0,2},{2,4},{4,6},{6,8},{8,10},{10,12},{12,14},{14,0},{1,3},{3,5},... | collective-permute-start | bytes 786440 | tf_op jit(solution)/shard_map/ppermute | solution.py:67
  30.9 123.5 %reduce-scatter.3.cloned.1.call-start = ((), (), s32[]{:S(2)}) async-start(), calls=%async_computation.5 | async-start | bytes 1572864 | tf_op jit(solution)/shard_map/reduce_scatter | solution.py:72
  45.9 9.1 %collective-permute-start.3 = (bf16[512,256]{1,0:T(8,128)(2,1)S(1)}, bf16[512,256]{1,0:T(8,128)(2,1)S(1)}, u32[]{:S(2)}, u32[]{:S(2)}) collective-permute-start(bf16[512,256]{1,0:T(8,128)(2,1)S(1)} %collective-permute-done.2), channel_id=1, source_target_pairs={{0,2},{2,4},{4,6},{6,8},{8,10},{10,12},{12,14},{14,0},{1,3},{3,5},... | collective-permute-start | bytes 786440 | tf_op jit(solution)/shard_map/ppermute | solution.py:67
  55.0 16.4 %collective-permute-start.4 = (bf16[512,256]{1,0:T(8,128)(2,1)S(1)}, bf16[512,256]{1,0:T(8,128)(2,1)S(1)}, u32[]{:S(2)}, u32[]{:S(2)}) collective-permute-start(bf16[512,256]{1,0:T(8,128)(2,1)S(1)} %collective-permute-done.3), channel_id=1, source_target_pairs={{0,2},{2,4},{4,6},{6,8},{8,10},{10,12},{12,14},{14,0},{1,3},{3,5},... | collective-permute-start | bytes 786440 | tf_op jit(solution)/shard_map/ppermute | solution.py:67
  71.3 15.9 %collective-permute-start.5 = (bf16[512,256]{1,0:T(8,128)(2,1)S(1)}, bf16[512,256]{1,0:T(8,128)(2,1)S(1)}, u32[]{:S(2)}, u32[]{:S(2)}) collective-permute-start(bf16[512,256]{1,0:T(8,128)(2,1)S(1)} %collective-permute-done.4), channel_id=1, source_target_pairs={{0,2},{2,4},{4,6},{6,8},{8,10},{10,12},{12,14},{14,0},{1,3},{3,5},... | collective-permute-start | bytes 786440 | tf_op jit(solution)/shard_map/ppermute | solution.py:67
  87.3 9.1 %collective-permute-start.6 = (bf16[512,256]{1,0:T(8,128)(2,1)S(1)}, bf16[512,256]{1,0:T(8,128)(2,1)S(1)}, u32[]{:S(2)}, u32[]{:S(2)}) collective-permute-start(bf16[512,256]{1,0:T(8,128)(2,1)S(1)} %collective-permute-done.5), channel_id=1, source_target_pairs={{0,2},{2,4},{4,6},{6,8},{8,10},{10,12},{12,14},{14,0},{1,3},{3,5},... | collective-permute-start | bytes 786440 | tf_op jit(solution)/shard_map/ppermute | solution.py:67
  88.8 19.6 %copy-start.3 = (bf16[256,1,2048]{2,0,1:T(8,128)(2,1)S(1)}, bf16[256,1,2048]{2,0,1:T(8,128)(2,1)}, u32[]{:S(2)}) copy-start(bf16[256,1,2048]{2,0,1:T(8,128)(2,1)} %all-gather.9.cloned.1.call-done) | copy-start | bytes 3145732
  88.8 19.6 %copy-start.6 = (f32[2048]{0:T(1024)S(1)}, f32[2048]{0:T(1024)}, u32[]{:S(2)}) copy-start(f32[2048]{0:T(1024)} %param.12) | copy-start | bytes 24580
  110.8 29.3 %copy-start.9 = (pred[8,36]{0,1:T(8,128)(4,1)S(1)}, pred[8,36]{0,1:T(8,128)(4,1)}, u32[]{:S(2)}) copy-start(pred[8,36]{0,1:T(8,128)(4,1)} %constant.59) | copy-start | bytes 868
  141.3 2.6 copy-start.8
  143.2 11.2 %copy-start.2 = (bf16[128,1,2048]{2,0,1:T(8,128)(2,1)S(1)}, bf16[128,1,2048]{2,0,1:T(8,128)(2,1)}, u32[]{:S(2)}) copy-start(bf16[128,1,2048]{2,0,1:T(8,128)(2,1)} %param.11) | copy-start | bytes 1572868
  147.3 121.4 %copy-start.7 = (f32[2048]{0:T(1024)S(1)}, f32[2048]{0:T(1024)}, u32[]{:S(2)}) copy-start(f32[2048]{0:T(1024)} %param.18) | copy-start | bytes 24580
  147.3 19.5 %all-gather.21.cloned.1.call-start = ((), (), s32[]{:S(2)}) async-start(), calls=%async_computation.10 | async-start | bytes 1572864 | tf_op jit(solution)/shard_map/all_gather | solution.py:80
  156.4 112.4 %all-gather.15.cloned.1.call-start = ((), (), s32[]{:S(2)}) async-start(), calls=%async_computation.6 | async-start | bytes 7077888 | tf_op jit(solution)/shard_map/all_gather | solution.py:87
  157.0 210.9 %all-gather.17.cloned.1.call-start = ((), (), s32[]{:S(2)}) async-start(), calls=%async_computation.7 | async-start | bytes 7077888 | tf_op jit(solution)/shard_map/all_gather | solution.py:88
  157.7 309.9 %all-gather.19.cloned.1.call-start = ((), (), s32[]{:S(2)}) async-start(), calls=%async_computation.8 | async-start | bytes 7077888 | tf_op jit(solution)/shard_map/all_gather | solution.py:94
  158.5 325.2 %reduce-scatter.5.cloned.1.call-start = ((), (), s32[]{:S(2)}) async-start(), calls=%async_computation.9 | async-start | bytes 1572864 | tf_op jit(solution)/shard_map/reduce_scatter | solution.py:96
  168.3 299.2 %copy-start.4 = (bf16[256,2048]{1,0:T(8,128)(2,1)S(1)}, bf16[256,2048]{1,0:T(8,128)(2,1)}, u32[]{:S(2)}) copy-start(bf16[256,2048]{1,0:T(8,128)(2,1)} %all-gather.21.cloned.1.call-done) | copy-start | bytes 3145732
  273.7 209.9 %copy-start.1 = (bf16[128,2048]{1,0:T(8,128)(2,1)S(1)}, bf16[128,2048]{1,0:T(8,128)(2,1)}, u32[]{:S(2)}) copy-start(bf16[128,2048]{1,0:T(8,128)(2,1)} %fusion.14) | copy-start | bytes 1572868
Sparse Core Ops, SparseCore 0:
  8.9 11.7 all-gather.8
  22.8 60.3 all-gather.12
  85.3 52.0 all-gather.10
  147.5 6.8 reduce-scatter.2
  156.5 10.2 all-gather.20
  168.8 99.8 all-gather.14
  270.9 96.8 all-gather.16
  369.9 97.6 all-gather.18
  477.0 6.5 reduce-scatter.4
